TPU v7x, 32 devices: a whole 2x2x4 slice. The times are simulated.
32 devices in a mesh: grp: 2 (over y), ep: 4 (over z), tp: 4 (over x, core).
Axes of the slice: x: 2, y: 2, z: 4, core: 2. Of those that a mesh axis runs over, the one named last changes fastest.
Arguments:
- queries: bfloat16 [2048, 2048], P(('grp', 'ep'), 'tp'), parts along dimension 0, may hold values from -8 to 8
- keys: bfloat16 [2048, 512], P(('grp', 'ep')), parts along dimension 0, may hold values from -8 to 8
- values: bfloat16 [2048, 512], P(('grp', 'ep')), parts along dimension 0, may hold values from -6 to 6
- q_gain: float32 [128], replicated, may hold values from 0.6 to 5.8
- k_gain: float32 [128], replicated, may hold values from 0.6 to 5.8
- w_out: bfloat16 [2048, 2048], P(None, 'tp'), may hold values from -0.125 to 0.125
- moe_rows: bfloat16 [1536, 2048], P(('grp', 'ep')), parts along dimension 0, may hold values from -6 to 6
- routes: int32 [1536, 2], P(('grp', 'ep')), parts along dimension 0, may hold values from 0 to 3, all different within a row; in each aligned block of 192 rows (0 to 191, 192 to 383, ...) at most 144 rows name the same one
- group_gate: float32 [1536], P(('grp', 'ep')), parts along dimension 0, may hold values from 0.25 to 1
- expert_logits: float32 [1536, 2], P(('grp', 'ep')), parts along dimension 0, may hold values from -6 to 6
- moe_gain: float32 [2048], replicated, may hold values from 0.1 to 1.9
- w_gate: bfloat16 [4, 2048, 2048], P('ep', None, 'tp'), may hold values from -0.125 to 0.125
- w_up: bfloat16 [4, 2048, 2048], P('ep', None, 'tp'), may hold values from -0.125 to 0.125
- w_down: bfloat16 [4, 2048, 2048], P('ep', 'tp'), may hold values from -0.125 to 0.125
Outputs:
- attn_out: bfloat16 [2048, 2048], P(('grp', 'ep'), 'tp'), parts along dimension 0
- moe_out: bfloat16 [1536, 2048], P(('grp', 'ep'), 'tp'), parts along dimension 0
There are 2 independent parts, one for each index of `grp`. A program takes and returns all parts, laid end to end along the dimension named above; an argument that names none is the same for every part. Nothing has to cross between parts.
Inputs may be any that keep to these rules, and one draw needn't show every extreme that they name: `routes`: each row names 2 different experts; within the rows of one index of ep no expert is named more than 144 times, a bound that some block reaches.
All inputs are finite; a program needn't handle non-finite values.
Results may differ from a plain program's by a relative error of at most 0.019.
The roundings to bfloat16 on the way count: a program that leaves them out, or rounds other values in their place, can miss the bound.
Values may be sent and summed in bfloat16 or wider, within the bound.
A program may use at most 64 MiB of HBM per device.

v0:
```python
import jax
import jax.numpy as jnp
from jax import lax
from jax.sharding import PartitionSpec as P

HEADS = 16
KV_HEADS = 4
HEAD_DIM = 128
GRID_W = 64
TOPK = 2


def head_norm(x, gain):
    wide = x.astype(jnp.float32)
    return wide * lax.rsqrt(jnp.mean(wide * wide, axis=-1, keepdims=True) + 1e-06) * gain


def rotate(x, first):
    count = x.shape[0]
    pos = first + jnp.arange(count, dtype=jnp.int32)
    row = (pos // GRID_W).astype(jnp.float32)
    col = (pos % GRID_W).astype(jnp.float32)
    nfreq = HEAD_DIM // 4
    inverse = 10000.0 ** (-jnp.arange(nfreq, dtype=jnp.float32) / nfreq)
    angle = jnp.concatenate(
        [
            row[:, None] * inverse,
            row[:, None] * inverse,
            col[:, None] * inverse,
            col[:, None] * inverse,
        ],
        axis=1,
    )
    parts = x.reshape(x.shape[:-1] + (2, 2, nfreq))
    turned = jnp.stack([-parts[..., 1, :], parts[..., 0, :]], axis=-2).reshape(x.shape)
    return x * jnp.cos(angle)[:, None, :] + turned * jnp.sin(angle)[:, None, :]


def per_device(
    queries,
    keys,
    values,
    q_gain,
    k_gain,
    w_out,
    moe_rows,
    routes,
    group_gate,
    expert_logits,
    moe_gain,
    w_gate,
    w_up,
    w_down,
):
    rows = queries.shape[0]
    heads_dev = queries.shape[1] // HEAD_DIM
    group = HEADS // KV_HEADS
    kv_dev = max(1, heads_dev // group)
    per_kv = heads_dev // kv_dev
    first_kv = lax.axis_index("tp") * heads_dev // group
    first_row = lax.axis_index("ep") * rows
    k_mine = lax.dynamic_slice_in_dim(keys, first_kv * HEAD_DIM, kv_dev * HEAD_DIM, 1)
    v_mine = lax.dynamic_slice_in_dim(values, first_kv * HEAD_DIM, kv_dev * HEAD_DIM, 1)
    k_rot = rotate(head_norm(k_mine.reshape(rows, kv_dev, HEAD_DIM), k_gain), first_row)
    k_rot = k_rot.astype(jnp.bfloat16).reshape(rows, kv_dev * HEAD_DIM)
    q_rot = rotate(head_norm(queries.reshape(rows, heads_dev, HEAD_DIM), q_gain), first_row)
    q_rot = q_rot.astype(jnp.bfloat16).reshape(rows, kv_dev, per_kv, HEAD_DIM)
    scale = HEAD_DIM ** (-0.5)
    top = jnp.full((rows, kv_dev, per_kv), -jnp.inf, jnp.float32)
    total = jnp.zeros((rows, kv_dev, per_kv), jnp.float32)
    acc = jnp.zeros((rows, kv_dev, per_kv, HEAD_DIM), jnp.float32)
    k_piece = lax.all_gather(k_rot, "ep", axis=0, tiled=True)
    v_piece = lax.all_gather(v_mine, "ep", axis=0, tiled=True)
    count = k_piece.shape[0]
    key_rows = k_piece.reshape(count, kv_dev, HEAD_DIM)
    value_rows = v_piece.reshape(count, kv_dev, HEAD_DIM)
    scores = (
        jnp.einsum("qkgd,nkd->qkgn", q_rot, key_rows, preferred_element_type=jnp.float32) * scale
    )
    new_top = jnp.max(scores, axis=-1)
    shrink = jnp.exp(top - new_top)
    expo = jnp.exp(scores - new_top[..., None])
    total = total * shrink + jnp.sum(expo, axis=-1)
    acc = acc * shrink[..., None] + jnp.einsum(
        "qkgn,nkd->qkgd", expo.astype(jnp.bfloat16), value_rows, preferred_element_type=jnp.float32
    )
    top, total, acc = (new_top, total, acc)
    mixed = (acc / total[..., None]).astype(jnp.bfloat16).reshape(rows, heads_dev * HEAD_DIM)
    attn_out = jnp.dot(
        lax.all_gather(mixed, "tp", axis=1, tiled=True), w_out, preferred_element_type=jnp.float32
    ).astype(jnp.bfloat16)
    count = moe_rows.shape[0]
    width = moe_rows.shape[1]
    peers = lax.axis_size("ep")
    capacity = 3 * count // peers
    wide = moe_rows.astype(jnp.float32)
    normed = (
        wide * lax.rsqrt(jnp.mean(wide * wide, axis=-1, keepdims=True) + 1e-06) * moe_gain
    ).astype(jnp.bfloat16)
    chosen = routes.reshape(-1)
    onehot = (chosen[:, None] == jnp.arange(peers, dtype=jnp.int32)[None, :]).astype(jnp.int32)
    rank = jnp.sum((jnp.cumsum(onehot, axis=0) - onehot) * onehot, axis=1)
    slots = chosen * capacity + rank
    owner = jnp.arange(count * TOPK, dtype=jnp.int32) // TOPK
    source = jnp.zeros((peers * capacity,), jnp.int32).at[slots].set(owner)
    used = jnp.zeros((peers * capacity,), jnp.bool_).at[slots].set(True)
    outgoing = jnp.where(used[:, None], normed[source], jnp.zeros((), jnp.bfloat16)).reshape(
        peers, capacity, width
    )
    part_cols = width // lax.axis_size("tp")
    mine = lax.dynamic_slice_in_dim(outgoing, lax.axis_index("tp") * part_cols, part_cols, 2)
    arrived = lax.all_gather(
        lax.all_to_all(mine, "ep", split_axis=0, concat_axis=0, tiled=True),
        "tp",
        axis=2,
        tiled=True,
    )
    first_dim, second_dim, cols = arrived.shape
    flat = arrived.reshape(first_dim * second_dim, cols)
    gate = jnp.dot(flat, w_gate[0], preferred_element_type=jnp.float32)
    up = jnp.dot(flat, w_up[0], preferred_element_type=jnp.float32)
    hidden = (jax.nn.silu(gate) * up).astype(jnp.bfloat16)
    result = jnp.dot(hidden, w_down[0], preferred_element_type=jnp.float32).astype(jnp.bfloat16)
    partial_value = result.reshape(first_dim, second_dim, cols)
    summed = (
        lax.psum_scatter(partial_value, "tp", scatter_dimension=2, tiled=True)
        .astype(jnp.float32)
        .astype(jnp.bfloat16)
    )
    back = lax.all_to_all(summed, "ep", split_axis=0, concat_axis=0, tiled=True)
    back = back.reshape(peers * capacity, back.shape[2])
    picked = back[slots].astype(jnp.float32).reshape(count, TOPK, back.shape[1])
    weights = group_gate[:, None] * jax.nn.softmax(expert_logits, axis=-1)
    moe_out = jnp.sum(weights[:, :, None] * picked, axis=1).astype(jnp.bfloat16)
    return (attn_out, moe_out)


def solution(mesh):
    placed = (
        P(("grp", "ep"), "tp"),
        P(("grp", "ep"), None),
        P(("grp", "ep"), None),
        P(),
        P(),
        P(None, "tp"),
        P(("grp", "ep"), None),
        P(("grp", "ep"), None),
        P(("grp", "ep")),
        P(("grp", "ep"), None),
        P(),
        P("ep", None, "tp"),
        P("ep", None, "tp"),
        P("ep", "tp", None),
    )
    return jax.shard_map(
        per_device,
        mesh=mesh,
        in_specs=placed,
        out_specs=(P(("grp", "ep"), "tp"), P(("grp", "ep"), "tp")),
        check_vma=False,
    )
```

profile of v0, /device:TPU:0, one launch (start us, length us, event | category | flops | bytes accessed | tf_op | source)
XLA Modules:
  0.0 148.1 jit_solution(11262557061539180350)
XLA Ops:
  7.2 0.9 copy.30
  9.2 1.2 reduce-window.6
  11.2 2.9 %scatter_custom_fusion.1 = s32[576]{0:T(1024)S(1)} fusion(s32[384]{0:T(512)S(1)} %fusion.58, s32[384]{0:T(512)S(1)} %add_select_fusion, s32[]{:T(128)} %constant.95.clone.1), kind=kCustom, calls=%fused_computation.81 | custom fusion | bytes 2308 | tf_op jit(solution)/shard_map/scatter | solution.py:105
  14.1 1.4 fusion.13
  15.5 2.0 %scatter_custom_fusion = pred[576]{0:T(1024)(128)(4,1)S(1)} fusion(s32[384]{0:T(512)S(1)} %fusion.58, pred[384]{0:T(512)(128)(4,1)S(1)} %broadcast.278, pred[]{:T(512)} %constant.115.clone.1), kind=kCustom, calls=%fused_computation.86 | custom fusion | bytes 577 | tf_op jit(solution)/shard_map/scatter | solution.py:106
  17.6 1.4 fusion.15
  19.0 4.0 %gather_fusion = bf16[576,2048]{1,0:T(8,128)(2,1)} fusion(bf16[192,2048]{1,0:T(8,128)(2,1)S(1)} %fusion.15, s32[1024]{0:T(1024)S(1)} %pad_clamp_fusion.1), kind=kCustom, calls=%fused_computation | custom fusion | bytes 4720896 | tf_op jit(solution)/shard_map/gather | solution.py:107
  23.0 1.3 dynamic-slice_select_fusion
  24.3 22.1 %all_to_all.10 = bf16[4,144,512]{2,1,0:T(8,128)(2,1)} all-to-all(bf16[4,144,512]{2,1,0:T(8,128)(2,1)S(1)} %dynamic-slice_select_fusion), channel_id=1, replica_groups=mesh['grp'=2,'ep'=4,'tp'=4] {'ep'}, dimensions={0} | all-to-all | bytes 1179648 | tf_op jit(solution)/shard_map/all_to_all | solution.py:113
  46.5 23.3 %all-gather.5.cloned.1.call-done = bf16[4,144,2048]{2,1,0:T(8,128)(2,1)} async-done(((bf16[4,144,512]{2,1,0:T(8,128)(2,1)}), bf16[4,144,2048]{2,1,0:T(8,128)(2,1)}) %all-gather.5.cloned.1.call-update) | async-done | bytes 2359312 | tf_op jit(solution)/shard_map/all_gather | solution.py:112
  69.7 4.7 %fusion.9 = f32[576,512]{1,0:T(8,128)} fusion(bf16[576,2048]{1,0:T(8,128)(2,1)} %bitcast.131, bf16[1,2048,512]{2,1,0:T(8,128)(2,1)} %param.25), kind=kOutput, calls=%fused_computation.15 | convolution fusion | flops 1207959552 | bytes 5636096 | tf_op jit(solution)/shard_map/dot_general | solution.py:120
  74.5 6.7 %convolution_convert_fusion = bf16[576,2048]{1,0:T(8,128)(2,1)} fusion(bf16[1,512,2048]{2,1,0:T(8,128)(2,1)S(1)} %copy-done, bf16[576,2048]{1,0:T(8,128)(2,1)} %bitcast.132, bf16[1,2048,512]{2,1,0:T(8,128)(2,1)} %param.26, f32[576,512]{1,0:T(8,128)} %fusion.9), kind=kOutput, calls=%fused_computation.9 | convolution fusion | flops 2418868224 | bytes 10092544 | tf_op jit(solution)/shard_map/dot_general | solution.py:123
  81.3 0.8 copy-done.2
  83.8 0.8 constant_dynamic-slice_fusion
  85.3 13.9 %all_gather.12 = bf16[1024,128]{1,0:T(8,128)(2,1)S(1)} all-gather(bf16[256,128]{1,0:T(8,128)(2,1)S(1)} %get-tuple-element.2), channel_id=1, replica_groups=mesh['grp'=2,'ep'=4,'tp'=4] {'ep'}, dimensions={0}, use_global_device_ids=true | all-gather | bytes 327680 | tf_op jit(solution)/shard_map/all_gather | solution.py:72
  99.2 14.7 %all_gather.13 = bf16[1024,128]{0,1:T(8,128)(2,1)S(1)} all-gather(bf16[256,128]{0,1:T(8,128)(2,1)S(1)} %copy.34), channel_id=1, replica_groups=mesh['grp'=2,'ep'=4,'tp'=4] {'ep'}, dimensions={0}, use_global_device_ids=true | all-gather | bytes 327680 | tf_op jit(solution)/shard_map/all_gather | solution.py:73
  113.9 0.7 bitcast_reduce_fusion
  114.6 0.7 fusion.1
  115.4 1.6 %fusion.31 = bf16[1,128,256,4]{2,1,3,0:T(8,128)(2,1)} fusion(f32[1024,256,4]{1,0,2:T(8,128)S(1)} %get-tuple-element.14, f32[256,4]{0,1:T(4,128)S(1)} %get-tuple-element.13, bf16[1024,128]{0,1:T(8,128)(2,1)S(1)} %all_gather.13, f32[256,4]{0,1:T(4,128)S(1)} %get-tuple-element.10, f32[256,4]{0,1:T(4,128)S(1)} %get-tuple-element.9), kind=kOutput, calls=%fused_computation.30 | convolution fusion | flops 271974400 | bytes 4730880 | tf_op jit(solution)/shard_map/qkgn,nkd->qkgd/dot_general | solution.py:84
  117.0 4.8 %all-to-all-start.1 = ((bf16[4,144,512]{2,1,0:T(8,128)(2,1)}), bf16[4,144,512]{2,1,0:T(8,128)(2,1)S(1)}, u32[]{:S(2)}, u32[]{:S(2)}) async-start(bf16[4,144,512]{2,1,0:T(8,128)(2,1)} %reduce-scatter.2.cloned.1.call-done), calls=%async_computation.2 | async-start | bytes 1179648 | tf_op jit(solution)/shard_map/all_to_all | solution.py:130
  122.0 12.0 %all-gather.3.cloned.1.call-done = bf16[256,2048]{0,1:T(8,128)(2,1)} async-done(((bf16[256,512]{0,1:T(8,128)(2,1)}), bf16[256,2048]{0,1:T(8,128)(2,1)}) %all-gather.3.cloned.1.call-update) | async-done | bytes 1048592 | tf_op jit(solution)/shard_map/all_gather | solution.py:90
  134.0 3.3 %convolution_convert_fusion.1 = bf16[256,512]{1,0:T(8,128)(2,1)} fusion(bf16[256,2048]{0,1:T(8,128)(2,1)} %all-gather.3.cloned.1.call-done, bf16[2048,512]{1,0:T(8,128)(2,1)} %param.19), kind=kOutput, calls=%fused_computation.28 | convolution fusion | flops 537001984 | bytes 3407872 | tf_op jit(solution)/shard_map/dot_general | solution.py:89
  137.3 2.1 %gather_fusion.1 = bf16[384,512]{1,0:T(8,128)(2,1)S(1)} fusion(bf16[576,512]{1,0:T(8,128)(2,1)S(1)} %bitcast.122, s32[1024]{0:T(1024)S(1)} %pad_clamp_fusion), kind=kCustom, calls=%fused_computation.1 | custom fusion | bytes 787968 | tf_op jit(solution)/shard_map/gather | solution.py:132
  139.9 1.7 %multiply_reduce_fusion = bf16[192,512]{1,0:T(8,128)(2,1)} fusion(f32[192,2,512]{2,1,0:T(2,128)S(1)} %reshape.352, f32[192,2]{1,0:T(8,128)S(1)} %copy.28), kind=kLoop, calls=%fused_computation.31 | loop fusion | flops 294912 | bytes 984576 | tf_op jit(solution)/shard_map/reduce_sum | solution.py:134
  (68 shorter events, 4.9 us)
Async XLA Ops:
  7.2 67.3 %copy-start = (bf16[1,512,2048]{2,1,0:T(8,128)(2,1)S(1)}, bf16[1,512,2048]{2,1,0:T(8,128)(2,1)}, u32[]{:S(2)}) copy-start(bf16[1,512,2048]{2,1,0:T(8,128)(2,1)} %param.27) | copy-start | bytes 6291460
  7.2 62.6 %all-gather.5.cloned.1.call-start = ((), (), s32[]{:S(2)}) async-start(), calls=%async_computation.4 | async-start | bytes 2949120 | tf_op jit(solution)/shard_map/all_gather | solution.py:112
  46.4 70.6 %reduce-scatter.2.cloned.1.call-start = ((), (), s32[]{:S(2)}) async-start(), calls=%async_computation.5 | async-start | bytes 2949120 | tf_op jit(solution)/shard_map/reduce_scatter | solution.py:126
  81.2 0.9 copy-start.2
  81.2 1.1 copy-start.4
  81.2 2.4 %copy-start.1 = (bf16[256,512]{1,0:T(8,128)(2,1)S(1)}, bf16[256,512]{1,0:T(8,128)(2,1)}, u32[]{:S(2)}) copy-start(bf16[256,512]{1,0:T(8,128)(2,1)} %param.14) | copy-start | bytes 786436
  81.2 2.5 %copy-start.5 = (f32[128]{0:T(128)S(1)}, f32[128]{0:T(128)}, u32[]{:S(2)}) copy-start(f32[128]{0:T(128)} %param.17) | copy-start | bytes 1540
  81.2 52.8 %all-gather.3.cloned.1.call-start = ((), (), s32[]{:S(2)}) async-start(), calls=%async_computation.3 | async-start | bytes 1310720 | tf_op jit(solution)/shard_map/all_gather | solution.py:90
  115.3 6.4 %copy-start.3 = (f32[192,2]{0,1:T(2,128)S(1)}, f32[192,2]{0,1:T(2,128)}, u32[]{:S(2)}) copy-start(f32[192,2]{0,1:T(2,128)} %param.23) | copy-start | bytes 4612
  115.3 6.5 %copy-start.6 = (f32[192]{0:T(256)S(1)}, f32[192]{0:T(256)}, u32[]{:S(2)}) copy-start(f32[192]{0:T(256)} %param.22) | copy-start | bytes 2308
  117.0 20.3 %all-to-all-start.1 = ((bf16[4,144,512]{2,1,0:T(8,128)(2,1)}), bf16[4,144,512]{2,1,0:T(8,128)(2,1)S(1)}, u32[]{:S(2)}, u32[]{:S(2)}) async-start(bf16[4,144,512]{2,1,0:T(8,128)(2,1)} %reduce-scatter.2.cloned.1.call-done), calls=%async_computation.2 | async-start | bytes 1179648 | tf_op jit(solution)/shard_map/all_to_all | solution.py:130
Sparse Core Ops, SparseCore 0:
  46.5 23.1 all-gather.4
  81.3 32.7 reduce-scatter.1
  117.1 16.8 all-gather.2
where the time goes:
time: 149 us; the launch traced here: 148 us
  blocking collectives  50.8 us (34%)
  waiting for transfers between devices  35.3 us (24%)
  matrix products  17.1 us (11%)
  local copies, waits for them, and re-layouts  15.8 us (11%)
  between operations  14.1 us (9%)
  other arithmetic  10.1 us (7%)
  starting transfers between devices  4.88 us (3%)
    all_gather x1, waiting for transfers between devices, per_device(): lax.all_gather(lax.all_to_all(mine, 'ep', split_axis=0, concat_axis=0, ti...  23.3 us
    all_to_all x1, blocking collectives, per_device(): lax.all_to_all(mine, 'ep', split_axis=0, concat_axis=0, tiled=True)  22.1 us
    all_gather x1, blocking collectives, per_device(): v_piece = lax.all_gather(v_mine, 'ep', axis=0, tiled=True)  14.7 us
    all_gather x1, blocking collectives, per_device(): k_piece = lax.all_gather(k_rot, 'ep', axis=0, tiled=True)  13.9 us
    all_gather x1, waiting for transfers between devices, per_device(): lax.all_gather(mixed, 'tp', axis=1, tiled=True)  12 us
    dot_general x1, matrix products, per_device(): jnp.dot(hidden, w_down[0], preferred_element_type=jnp.float32)  6.71 us
    all_to_all x1, starting transfers between devices, per_device(): back = lax.all_to_all(summed, 'ep', split_axis=0, concat_axis=0, tiled=True)  4.76 us
    dot_general x1, matrix products, per_device(): gate = jnp.dot(flat, w_gate[0], preferred_element_type=jnp.float32)  4.74 us
  transfers between devices with their start and end apart: 4, of which 2 were waited for; matrix products, arithmetic and copies ran while one was open for 6% of the time, Pallas kernels for 0%

commit v1 on v0

--- a/solution.py
+++ b/solution.py
@@ -69,7 +69,12 @@
     top = jnp.full((rows, kv_dev, per_kv), -jnp.inf, jnp.float32)
     total = jnp.zeros((rows, kv_dev, per_kv), jnp.float32)
     acc = jnp.zeros((rows, kv_dev, per_kv, HEAD_DIM), jnp.float32)
-    k_piece = lax.all_gather(k_rot, "ep", axis=0, tiled=True)
+    ring = [k_rot]
+    for hop in range(3):
+        ring.append(lax.ppermute(ring[-1], "ep", [(dev, (dev + 1) % 4) for dev in range(4)]))
+    k_piece = jnp.roll(
+        jnp.concatenate(ring[::-1], axis=0), (lax.axis_index("ep") + 1) * ring[0].shape[0], axis=0
+    )
     v_piece = lax.all_gather(v_mine, "ep", axis=0, tiled=True)
     count = k_piece.shape[0]
     key_rows = k_piece.reshape(count, kv_dev, HEAD_DIM)

time: 149 us -> 148 us (level)
  blocking collectives: 50.8 us -> 36.3 us
  waiting for transfers between devices: 35.3 us -> 47.5 us
    all_gather x1 -> x0, blocking collectives: 13.9 us -> none  [per_device(): k_piece = lax.all_gather(k_rot, 'ep', axis=0, tiled=True)]
    ppermute x0 -> x3, waiting for transfers between devices: none -> 8.75 us  [per_device(): lax.ppermute(ring[-1], 'ep', [(dev, (dev + 1) % 4) for dev in range(4)])]
    all_gather x1, waiting for transfers between devices: 12 us -> 14.1 us  [per_device(): lax.all_gather(mixed, 'tp', axis=1, tiled=True)]
    reduce_scatter x1, waiting for transfers between devices: 0.02 us -> 1.57 us  [per_device(): lax.psum_scatter(partial_value, 'tp', scatter_dimension=2, tiled=True)]
    ppermute x0 -> x3, starting transfers between devices: none -> 1.54 us  [per_device(): lax.ppermute(ring[-1], 'ep', [(dev, (dev + 1) % 4) for dev in range(4)])]
  transfers between devices with their start and end apart: 4 -> 7, of which waited for: 2 -> 5; matrix products, arithmetic and copies ran while one was open for 6% -> 7% of each run, Pallas kernels for 0% -> 0%
where the time goes in v1:
time: 148 us; the launch traced here: 147 us
  waiting for transfers between devices  47.5 us (32%)
  blocking collectives  36.3 us (25%)
  matrix products  17.1 us (12%)
  local copies, waits for them, and re-layouts  15.6 us (11%)
  between operations  14.2 us (10%)
  other arithmetic  10.2 us (7%)
  starting transfers between devices  6.26 us (4%)
    all_gather x1, waiting for transfers between devices, per_device(): lax.all_gather(lax.all_to_all(mine, 'ep', split_axis=0, concat_axis=0, ti...  23.1 us
    all_to_all x1, blocking collectives, per_device(): lax.all_to_all(mine, 'ep', split_axis=0, concat_axis=0, tiled=True)  22.1 us
    all_gather x1, blocking collectives, per_device(): v_piece = lax.all_gather(v_mine, 'ep', axis=0, tiled=True)  14.2 us
    all_gather x1, waiting for transfers between devices, per_device(): lax.all_gather(mixed, 'tp', axis=1, tiled=True)  14.1 us
    ppermute x3, waiting for transfers between devices, per_device(): lax.ppermute(ring[-1], 'ep', [(dev, (dev + 1) % 4) for dev in range(4)])  8.75 us
    dot_general x1, matrix products, per_device(): jnp.dot(hidden, w_down[0], preferred_element_type=jnp.float32)  6.71 us
    dot_general x1, matrix products, per_device(): gate = jnp.dot(flat, w_gate[0], preferred_element_type=jnp.float32)  4.74 us
    all_to_all x1, starting transfers between devices, per_device(): back = lax.all_to_all(summed, 'ep', split_axis=0, concat_axis=0, tiled=True)  4.6 us
  transfers between devices with their start and end apart: 7, of which 5 were waited for; matrix products, arithmetic and copies ran while one was open for 7% of the time, Pallas kernels for 0%

profile of v1, /device:TPU:0, one launch (start us, length us, event | category | flops | bytes accessed | tf_op | source)
XLA Modules:
  0.0 147.2 jit_solution(12162952591111411645)
XLA Ops:
  7.2 0.9 copy.30
  9.2 1.2 reduce-window.6
  11.2 2.9 %scatter_custom_fusion.1 = s32[576]{0:T(1024)S(1)} fusion(s32[384]{0:T(512)S(1)} %fusion.59, s32[384]{0:T(512)S(1)} %add_select_fusion, s32[]{:T(128)} %constant.114.clone.1), kind=kCustom, calls=%fused_computation.90 | custom fusion | bytes 2308 | tf_op jit(solution)/shard_map/scatter | solution.py:110
  14.1 1.4 fusion.13
  15.5 2.0 %scatter_custom_fusion = pred[576]{0:T(1024)(128)(4,1)S(1)} fusion(s32[384]{0:T(512)S(1)} %fusion.59, pred[384]{0:T(512)(128)(4,1)S(1)} %broadcast.285, pred[]{:T(512)} %constant.137.clone.1), kind=kCustom, calls=%fused_computation.95 | custom fusion | bytes 577 | tf_op jit(solution)/shard_map/scatter | solution.py:111
  17.6 1.4 fusion.15
  19.0 4.0 %gather_fusion = bf16[576,2048]{1,0:T(8,128)(2,1)} fusion(bf16[192,2048]{1,0:T(8,128)(2,1)S(1)} %fusion.15, s32[1024]{0:T(1024)S(1)} %pad_clamp_fusion.1), kind=kCustom, calls=%fused_computation | custom fusion | bytes 4720896 | tf_op jit(solution)/shard_map/gather | solution.py:112
  23.0 1.3 dynamic-slice_select_fusion
  24.3 22.1 %all_to_all.10 = bf16[4,144,512]{2,1,0:T(8,128)(2,1)} all-to-all(bf16[4,144,512]{2,1,0:T(8,128)(2,1)S(1)} %dynamic-slice_select_fusion), channel_id=1, replica_groups=mesh['grp'=2,'ep'=4,'tp'=4] {'ep'}, dimensions={0} | all-to-all | bytes 1179648 | tf_op jit(solution)/shard_map/all_to_all | solution.py:118
  46.7 23.1 %all-gather.5.cloned.1.call-done = bf16[4,144,2048]{2,1,0:T(8,128)(2,1)} async-done(((bf16[4,144,512]{2,1,0:T(8,128)(2,1)}), bf16[4,144,2048]{2,1,0:T(8,128)(2,1)}) %all-gather.5.cloned.1.call-update) | async-done | bytes 2359312 | tf_op jit(solution)/shard_map/all_gather | solution.py:117
  69.8 4.7 %fusion.9 = f32[576,512]{1,0:T(8,128)} fusion(bf16[576,2048]{1,0:T(8,128)(2,1)} %bitcast.131, bf16[1,2048,512]{2,1,0:T(8,128)(2,1)} %param.25), kind=kOutput, calls=%fused_computation.15 | convolution fusion | flops 1207959552 | bytes 5636096 | tf_op jit(solution)/shard_map/dot_general | solution.py:125
  74.5 6.7 %convolution_convert_fusion = bf16[576,2048]{1,0:T(8,128)(2,1)} fusion(bf16[1,512,2048]{2,1,0:T(8,128)(2,1)S(1)} %copy-done, bf16[576,2048]{1,0:T(8,128)(2,1)} %bitcast.132, bf16[1,2048,512]{2,1,0:T(8,128)(2,1)} %param.26, f32[576,512]{1,0:T(8,128)} %fusion.9), kind=kOutput, calls=%fused_computation.9 | convolution fusion | flops 2418868224 | bytes 10092544 | tf_op jit(solution)/shard_map/dot_general | solution.py:128
  83.0 1.5 %collective-permute-start = (bf16[256,128]{1,0:T(8,128)(2,1)S(1)}, bf16[256,128]{1,0:T(8,128)(2,1)S(1)}, u32[]{:S(2)}, u32[]{:S(2)}) collective-permute-start(bf16[256,128]{1,0:T(8,128)(2,1)S(1)} %get-tuple-element.2), channel_id=1, source_target_pairs={{0,4},{4,8},{8,12},{12,0},{1,5},{5,9},{9,13},{13,1},{2,6},{6,10},{... | collective-permute-start | bytes 196616 | tf_op jit(solution)/shard_map/ppermute | solution.py:74
  85.2 0.9 constant_dynamic-slice_fusion
  86.2 2.9 %collective-permute-done = bf16[256,128]{1,0:T(8,128)(2,1)S(1)} collective-permute-done((bf16[256,128]{1,0:T(8,128)(2,1)S(1)}, bf16[256,128]{1,0:T(8,128)(2,1)S(1)}, u32[]{:S(2)}, u32[]{:S(2)}) %collective-permute-start) | collective-permute-done | bytes 65568 | tf_op jit(solution)/shard_map/ppermute | solution.py:74
  89.3 5.8 %collective-permute-done.1 = bf16[256,128]{1,0:T(8,128)(2,1)S(1)} collective-permute-done((bf16[256,128]{1,0:T(8,128)(2,1)S(1)}, bf16[256,128]{1,0:T(8,128)(2,1)S(1)}, u32[]{:S(2)}, u32[]{:S(2)}) %collective-permute-start.1) | collective-permute-done | bytes 65568 | tf_op jit(solution)/shard_map/ppermute | solution.py:74
  95.2 14.2 %all_gather.9 = bf16[1024,128]{0,1:T(8,128)(2,1)S(1)} all-gather(bf16[256,128]{0,1:T(8,128)(2,1)S(1)} %copy.34), channel_id=1, replica_groups=mesh['grp'=2,'ep'=4,'tp'=4] {'ep'}, dimensions={0}, use_global_device_ids=true | all-gather | bytes 327680 | tf_op jit(solution)/shard_map/all_gather | solution.py:78
  111.0 1.6 %fusion.31 = bf16[1,128,256,4]{2,1,3,0:T(8,128)(2,1)} fusion(f32[1024,256,4]{1,0,2:T(8,128)S(1)} %get-tuple-element.14, f32[256,4]{0,1:T(4,128)S(1)} %get-tuple-element.13, bf16[1024,128]{0,1:T(8,128)(2,1)S(1)} %all_gather.9, f32[256,4]{0,1:T(4,128)S(1)} %get-tuple-element.10, f32[256,4]{0,1:T(4,128)S(1)} %get-tuple-element.9), kind=kOutput, calls=%fused_computation.30 | convolution fusion | flops 271974400 | bytes 4730880 | tf_op jit(solution)/shard_map/qkgn,nkd->qkgd/dot_general | solution.py:89
  112.6 1.6 %reduce-scatter.2.cloned.1.call-done = bf16[4,144,512]{2,1,0:T(8,128)(2,1)} async-done(((bf16[4,144,2048]{2,1,0:T(8,128)(2,1)}), bf16[4,144,512]{2,1,0:T(8,128)(2,1)}) %reduce-scatter.2.cloned.1.call-update) | async-done | bytes 589840 | tf_op jit(solution)/shard_map/reduce_scatter | solution.py:131
  114.2 4.6 %all-to-all-start.1 = ((bf16[4,144,512]{2,1,0:T(8,128)(2,1)}), bf16[4,144,512]{2,1,0:T(8,128)(2,1)S(1)}, u32[]{:S(2)}, u32[]{:S(2)}) async-start(bf16[4,144,512]{2,1,0:T(8,128)(2,1)} %reduce-scatter.2.cloned.1.call-done), calls=%async_computation.2 | async-start | bytes 1179648 | tf_op jit(solution)/shard_map/all_to_all | solution.py:135
  119.0 14.1 %all-gather.3.cloned.1.call-done = bf16[256,2048]{0,1:T(8,128)(2,1)} async-done(((bf16[256,512]{0,1:T(8,128)(2,1)}), bf16[256,2048]{0,1:T(8,128)(2,1)}) %all-gather.3.cloned.1.call-update) | async-done | bytes 1048592 | tf_op jit(solution)/shard_map/all_gather | solution.py:95
  133.0 3.3 %convolution_convert_fusion.1 = bf16[256,512]{1,0:T(8,128)(2,1)} fusion(bf16[256,2048]{0,1:T(8,128)(2,1)} %all-gather.3.cloned.1.call-done, bf16[2048,512]{1,0:T(8,128)(2,1)} %param.19), kind=kOutput, calls=%fused_computation.28 | convolution fusion | flops 537001984 | bytes 3407872 | tf_op jit(solution)/shard_map/dot_general | solution.py:94
  136.4 2.1 %gather_fusion.1 = bf16[384,512]{1,0:T(8,128)(2,1)S(1)} fusion(bf16[576,512]{1,0:T(8,128)(2,1)S(1)} %bitcast.122, s32[1024]{0:T(1024)S(1)} %pad_clamp_fusion), kind=kCustom, calls=%fused_computation.1 | custom fusion | bytes 787968 | tf_op jit(solution)/shard_map/gather | solution.py:137
  139.0 1.7 %multiply_reduce_fusion = bf16[192,512]{1,0:T(8,128)(2,1)} fusion(f32[192,2,512]{2,1,0:T(2,128)S(1)} %reshape.352, f32[192,2]{1,0:T(8,128)S(1)} %copy.28), kind=kLoop, calls=%fused_computation.31 | loop fusion | flops 294912 | bytes 984576 | tf_op jit(solution)/shard_map/reduce_sum | solution.py:139
  (81 shorter events, 7.0 us)
Async XLA Ops:
  7.2 67.4 %copy-start = (bf16[1,512,2048]{2,1,0:T(8,128)(2,1)S(1)}, bf16[1,512,2048]{2,1,0:T(8,128)(2,1)}, u32[]{:S(2)}) copy-start(bf16[1,512,2048]{2,1,0:T(8,128)(2,1)} %param.27) | copy-start | bytes 6291460
  7.2 62.6 %all-gather.5.cloned.1.call-start = ((), (), s32[]{:S(2)}) async-start(), calls=%async_computation.4 | async-start | bytes 2949120 | tf_op jit(solution)/shard_map/all_gather | solution.py:117
  23.0 23.6 %copy-start.2 = (bf16[256,512]{1,0:T(8,128)(2,1)S(1)}, bf16[256,512]{1,0:T(8,128)(2,1)}, u32[]{:S(2)}) copy-start(bf16[256,512]{1,0:T(8,128)(2,1)} %param.15) | copy-start | bytes 786436
  46.5 67.7 %reduce-scatter.2.cloned.1.call-start = ((), (), s32[]{:S(2)}) async-start(), calls=%async_computation.5 | async-start | bytes 2949120 | tf_op jit(solution)/shard_map/reduce_scatter | solution.py:131
  81.2 0.7 copy-start.4
  81.2 3.5 %copy-start.1 = (bf16[256,512]{1,0:T(8,128)(2,1)S(1)}, bf16[256,512]{1,0:T(8,128)(2,1)}, u32[]{:S(2)}) copy-start(bf16[256,512]{1,0:T(8,128)(2,1)} %param.14) | copy-start | bytes 786436
  81.3 3.6 %copy-start.5 = (f32[128]{0:T(128)S(1)}, f32[128]{0:T(128)}, u32[]{:S(2)}) copy-start(f32[128]{0:T(128)} %param.17) | copy-start | bytes 1540
  81.3 51.8 %all-gather.3.cloned.1.call-start = ((), (), s32[]{:S(2)}) async-start(), calls=%async_computation.3 | async-start | bytes 1310720 | tf_op jit(solution)/shard_map/all_gather | solution.py:95
  83.0 6.1 %collective-permute-start = (bf16[256,128]{1,0:T(8,128)(2,1)S(1)}, bf16[256,128]{1,0:T(8,128)(2,1)S(1)}, u32[]{:S(2)}, u32[]{:S(2)}) collective-permute-start(bf16[256,128]{1,0:T(8,128)(2,1)S(1)} %get-tuple-element.2), channel_id=1, source_target_pairs={{0,4},{4,8},{8,12},{12,0},{1,5},{5,9},{9,13},{13,1},{2,6},{6,10},{... | collective-permute-start | bytes 196616 | tf_op jit(solution)/shard_map/ppermute | solution.py:74
  89.1 6.1 %collective-permute-start.1 = (bf16[256,128]{1,0:T(8,128)(2,1)S(1)}, bf16[256,128]{1,0:T(8,128)(2,1)S(1)}, u32[]{:S(2)}, u32[]{:S(2)}) collective-permute-start(bf16[256,128]{1,0:T(8,128)(2,1)S(1)} %collective-permute-done), channel_id=1, source_target_pairs={{0,4},{4,8},{8,12},{12,0},{1,5},{5,9},{9,13},{13,1},{2,6},{6,10},{... | collective-permute-start | bytes 196616 | tf_op jit(solution)/shard_map/ppermute | solution.py:74
  95.2 14.2 %collective-permute-start.2 = (bf16[256,128]{1,0:T(8,128)(2,1)S(1)}, bf16[256,128]{1,0:T(8,128)(2,1)S(1)}, u32[]{:S(2)}, u32[]{:S(2)}) collective-permute-start(bf16[256,128]{1,0:T(8,128)(2,1)S(1)} %collective-permute-done.1), channel_id=1, source_target_pairs={{0,4},{4,8},{8,12},{12,0},{1,5},{5,9},{9,13},{13,1},{2,6},{6,10},{... | collective-permute-start | bytes 196616 | tf_op jit(solution)/shard_map/ppermute | solution.py:74
  111.0 7.8 %copy-start.3 = (f32[192,2]{0,1:T(2,128)S(1)}, f32[192,2]{0,1:T(2,128)}, u32[]{:S(2)}) copy-start(f32[192,2]{0,1:T(2,128)} %param.23) | copy-start | bytes 4612
  111.0 7.9 %copy-start.6 = (f32[192]{0:T(256)S(1)}, f32[192]{0:T(256)}, u32[]{:S(2)}) copy-start(f32[192]{0:T(256)} %param.22) | copy-start | bytes 2308
  114.2 22.2 %all-to-all-start.1 = ((bf16[4,144,512]{2,1,0:T(8,128)(2,1)}), bf16[4,144,512]{2,1,0:T(8,128)(2,1)S(1)}, u32[]{:S(2)}, u32[]{:S(2)}) async-start(bf16[4,144,512]{2,1,0:T(8,128)(2,1)} %reduce-scatter.2.cloned.1.call-done), calls=%async_computation.2 | async-start | bytes 1179648 | tf_op jit(solution)/shard_map/all_to_all | solution.py:135
Sparse Core Ops, SparseCore 0:
  46.6 23.1 all-gather.4
  81.4 32.7 reduce-scatter.1
  116.3 16.6 all-gather.2
